TPU v7x, 32 devices: a whole 2x2x4 slice. The times are simulated.
32 devices in a mesh: fs: 16 (over z, y, core), tp: 2 (over x).
Axes of the slice: x: 2, y: 2, z: 4, core: 2. Of those that a mesh axis runs over, the one named last changes fastest.
Arguments:
- inputs: bfloat16 [32768, 2048], P('fs'), may hold values from -6 to 6
- key_grads: bfloat16 [32768, 1024], P('fs', 'tp'), may hold values from -0.078125 to 0.078125
- weights: float32 [2048, 1024], P('fs', 'tp'), may hold values from -6 to 6
- momentum: float32 [2048, 1024], P('fs', 'tp'), may hold values from -6 to 6
- left_stat: float32 [4, 2048, 2048], P('tp', 'fs'), may hold values from -96 to 96
- right_stat: float32 [8, 128, 128], P('tp'), may hold values from -256 to 256
- left_root: bfloat16 [4, 2048, 2048], P('tp', 'fs'), may hold values from -0.125 to 0.125
- right_root: bfloat16 [8, 128, 128], P('tp'), may hold values from -0.5 to 0.5
Outputs:
- momentum_next: float32 [2048, 1024], P('fs', 'tp')
- left_next: float32 [4, 2048, 2048], P('tp', 'fs')
- right_next: float32 [8, 128, 128], P('tp')
- update: float32 [2048, 1024], P('fs', 'tp')
- weights_next: float32 [2048, 1024], P('fs', 'tp')
- weights_copy: bfloat16 [2048, 1024], P(None, 'tp')
All inputs are finite; a program needn't handle non-finite values.
Results may differ from a plain program's by a relative error of at most 0.0033.
Values may be sent and summed in bfloat16 or wider, within the bound.
A program may use at most 64 MiB of HBM per device.

v0:
```python
import jax
import jax.numpy as jnp
from jax import lax
from jax.sharding import PartitionSpec as P


def body(inputs, key_grads, weights, momentum, left_stat, right_stat, left_root, right_root):
    row_count = weights.shape[0]
    col_count = weights.shape[1]
    block_count = left_root.shape[0]
    head_count = right_root.shape[0]
    head_size = right_root.shape[1]
    model_width = inputs.shape[1]
    partial_grad = lax.dot_general(
        inputs, key_grads, (((0,), (0,)), ((), ())), preferred_element_type=jnp.float32
    )
    summed = lax.psum(partial_grad, "fs")
    whole_bf = summed.astype(jnp.bfloat16)
    row_offset = lax.axis_index("fs") * row_count
    grad = lax.dynamic_slice_in_dim(summed, row_offset, row_count, 0)
    own_rows = lax.dynamic_slice_in_dim(whole_bf, row_offset, row_count, 0)
    whole_blocks = whole_bf.reshape(model_width, block_count, -1)
    left_part = jnp.einsum(
        "brd,dbc->rbc", left_root, whole_blocks, preferred_element_type=jnp.float32
    ).reshape(row_count, col_count)
    row_gram = jnp.einsum(
        "rbc,dbc->brd",
        own_rows.reshape(row_count, block_count, -1),
        whole_blocks,
        preferred_element_type=jnp.float32,
    )
    whole_heads = whole_bf.reshape(model_width, head_count, head_size)
    head_gram = jnp.einsum(
        "dhi,dhj->hij", whole_heads, whole_heads, preferred_element_type=jnp.float32
    )
    left_bf = left_part.astype(jnp.bfloat16)
    precond = jnp.einsum(
        "rhi,hij->rhj",
        left_bf.reshape(row_count, head_count, head_size),
        right_root,
        preferred_element_type=jnp.float32,
    ).reshape(row_count, col_count)
    left_next = 0.95 * left_stat + 0.05 * row_gram
    right_next = 0.95 * right_stat + 0.05 * head_gram
    grad_square, precond_square = lax.psum(
        (jnp.sum(grad * grad), jnp.sum(precond * precond)), ("fs", "tp")
    )
    scale = jnp.sqrt(grad_square / (precond_square + 1e-06))
    momentum_next = 0.9 * momentum + scale * precond
    update = -0.25 * (momentum_next + 0.4 * weights)
    weights_next = weights + update
    weights_copy = lax.all_gather(weights_next.astype(jnp.bfloat16), "fs", axis=0, tiled=True)
    return (momentum_next, left_next, right_next, update, weights_next, weights_copy)


def solution(mesh):
    in_specs = (
        P("fs", None),
        P("fs", "tp"),
        P("fs", "tp"),
        P("fs", "tp"),
        P("tp", "fs", None),
        P("tp", None, None),
        P("tp", "fs", None),
        P("tp", None, None),
    )
    out_specs = (
        P("fs", "tp"),
        P("tp", "fs", None),
        P("tp", None, None),
        P("fs", "tp"),
        P("fs", "tp"),
        P(None, "tp"),
    )
    return jax.shard_map(body, mesh=mesh, in_specs=in_specs, out_specs=out_specs, check_vma=False)
```

profile of v0, /device:TPU:0, one launch (start us, length us, event | category | flops | bytes accessed | tf_op | source)
XLA Modules:
  0.0 232.3 jit_solution(892505422793026913)
XLA Ops:
  7.2 0.0 copy-start
  7.2 0.0 all-reduce.3.cloned.1.call-start
  7.2 1.5 copy-done
  8.8 9.8 %fusion.19 = f32[2048,512]{1,0:T(8,128)} fusion(bf16[2048,2048]{1,0:T(8,128)(2,1)} %param.8, bf16[2048,512]{1,0:T(8,128)(2,1)S(1)} %copy-done), kind=kOutput, calls=%fused_computation.20 | convolution fusion | flops 4294967296 | bytes 14680064 | tf_op jit(solution)/shard_map/dot_general | solution.py:14
  18.6 0.0 all-reduce.3.cloned.1.call-update
  18.6 0.0 all-gather.2.cloned.1.call-start
  18.6 113.9 %all-reduce.3.cloned.1.call-done = f32[2048,512]{1,0:T(8,128)} async-done(((f32[2048,512]{1,0:T(8,128)}), f32[2048,512]{1,0:T(8,128)}) %all-reduce.3.cloned.1.call-update) | async-done | bytes 4194320 | tf_op jit(solution)/shard_map/psum | solution.py:17
  132.6 0.0 copy-start.8
  132.6 2.5 %convert_element_type.16 = bf16[2048,512]{1,0:T(8,128)(2,1)S(1)} convert(f32[2048,512]{1,0:T(8,128)} %all-reduce.3.cloned.1.call-done) | non-fusion elementwise | flops 1048576 | bytes 6291456 | tf_op jit(solution)/shard_map/convert_element_type | solution.py:18
  135.1 0.0 copy-start.1
  135.1 0.0 copy-start.7
  135.2 0.0 copy-done.8
  135.2 0.0 copy-start.5
  135.2 0.0 copy-start.6
  135.2 0.9 fusion.15
  136.1 0.1 copy-done.7
  136.2 0.0 copy-start.4
  136.2 0.9 multiply_reduce_fusion
  137.1 0.0 copy-done.1
  137.1 1.6 multiply_reduce_fusion.1
  138.7 39.7 %all-reduce = (f32[]{:T(128)}, f32[]{:T(128)}) all-reduce(f32[]{:T(128)} %multiply_reduce_fusion.1, f32[]{:T(128)} %get-tuple-element.12), channel_id=1, replica_groups=mesh['fs'=16,'tp'=2] {'fs','tp'}, use_global_device_ids=true, to_apply=%region_2.0 | all-reduce | flops 2 | bytes 16 | tf_op jit(solution)/shard_map/psum | solution.py:45
  179.8 0.1 copy.24
  179.9 0.0 copy-done.5
  179.9 0.0 copy-done.6
  179.9 1.0 fusion.18
  181.0 0.0 all-gather.2.cloned.1.call-update
  181.0 0.9 constant_dynamic-slice_fusion
  181.9 0.1 copy.25
  182.0 0.0 copy-done.4
  182.0 0.0 copy-start.2
  182.1 0.0 copy-start.3
  182.1 5.6 %fusion.12 = f32[4,128,128]{2,1,0:T(8,128)} fusion(f32[4,128,128]{2,1,0:T(8,128)S(1)} %copy-done.4, f32[2048,512]{1,0:T(8,128)} %all-reduce.3.cloned.1.call-done), kind=kOutput, calls=%fused_computation.11 | convolution fusion | flops 269680640 | bytes 4718592 | tf_op jit(solution)/shard_map/dhi,dhj->hij/dot_general | solution.py:33
  187.7 0.0 copy-done.2
  187.7 0.0 copy-done.3
  187.7 2.2 fusion
  189.9 32.6 %all-gather.2.cloned.1.call-done = bf16[2048,512]{1,0:T(8,128)(2,1)} async-done(((bf16[128,512]{1,0:T(8,128)(2,1)}), bf16[2048,512]{1,0:T(8,128)(2,1)}) %all-gather.2.cloned.1.call-update) | async-done | bytes 2097168 | tf_op jit(solution)/shard_map/all_gather | solution.py:52
  222.4 3.0 %copy.55 = bf16[2048,512]{1,0:T(8,128)(2,1)} copy(bf16[2048,512]{1,0:T(8,128)(2,1)} %all-gather.2.cloned.1.call-done) | data formatting | bytes 4194304
  (1 shorter events, 0.0 us)
Async XLA Ops:
  7.2 1.6 copy-start
  7.2 125.4 %all-reduce.3.cloned.1.call-start = ((), (), s32[]{:S(2)}) async-start(), calls=%async_computation | async-start | bytes 8388608 | tf_op jit(solution)/shard_map/psum | solution.py:17
  18.6 203.8 %all-gather.2.cloned.1.call-start = ((), (), s32[]{:S(2)}) async-start(), calls=%async_computation.1 | async-start | bytes 2228224 | tf_op jit(solution)/shard_map/all_gather | solution.py:52
  132.6 2.6 %copy-start.8 = (bf16[2,128,2048]{2,1,0:T(8,128)(2,1)S(1)}, bf16[2,128,2048]{2,1,0:T(8,128)(2,1)}, u32[]{:S(2)}) copy-start(bf16[2,128,2048]{2,1,0:T(8,128)(2,1)} %param.14) | copy-start | bytes 3145732
  135.1 1.9 copy-start.1
  135.1 1.0 copy-start.7
  135.2 44.7 %copy-start.5 = (f32[128,512]{1,0:T(8,128)S(1)}, f32[128,512]{1,0:T(8,128)}, u32[]{:S(2)}) copy-start(f32[128,512]{1,0:T(8,128)} %param.10) | copy-start | bytes 786436
  135.2 44.7 %copy-start.6 = (f32[128,512]{1,0:T(8,128)S(1)}, f32[128,512]{1,0:T(8,128)}, u32[]{:S(2)}) copy-start(f32[128,512]{1,0:T(8,128)} %param.11) | copy-start | bytes 786436
  136.2 45.8 %copy-start.4 = (f32[4,128,128]{2,1,0:T(8,128)S(1)}, f32[4,128,128]{2,1,0:T(8,128)}, u32[]{:S(2)}) copy-start(f32[4,128,128]{2,1,0:T(8,128)} %param.13) | copy-start | bytes 786436
  182.0 5.6 %copy-start.2 = (bf16[2048,512]{1,0:T(8,128)(2,1)S(1)}, bf16[2048,512]{1,0:T(8,128)(2,1)}, u32[]{:S(2)}) copy-start(bf16[2048,512]{1,0:T(8,128)(2,1)} %copy-done.1) | copy-start | bytes 6291460
  182.1 5.6 %copy-start.3 = (f32[2,128,2048]{2,1,0:T(8,128)S(1)}, f32[2,128,2048]{2,1,0:T(8,128)}, u32[]{:S(2)}) copy-start(f32[2,128,2048]{2,1,0:T(8,128)} %param.12) | copy-start | bytes 6291460
Sparse Core Ops, SparseCore 0:
  18.7 113.8 all-reduce.2
  181.1 41.2 all-gather.1
where the time goes:
time: 233 us; the launch traced here: 232 us
  waiting for transfers between devices  147 us (63%)
  blocking collectives  39.7 us (17%)
  matrix products  19.4 us (8%)
  between operations  15.5 us (7%)
  local copies, waits for them, and re-layouts  5.87 us (3%)
  other arithmetic  5.21 us (2%)
    psum x1, waiting for transfers between devices, body(): summed = lax.psum(partial_grad, 'fs')  114 us
    psum x1, blocking collectives, body(): lax.psum((jnp.sum(grad * grad), jnp.sum(precond * precond)), ('fs', 'tp'))  39.7 us
    all_gather x1, waiting for transfers between devices, body(): lax.all_gather(weights_next.astype(jnp.bfloat16), 'fs', axis=0, tiled=True)  32.6 us
    dot_general x1, matrix products, body(): lax.dot_general(inputs, key_grads, (((0,), (0,)), ((), ())), preferred_el...  9.81 us
    dot_general x1, matrix products, body(): jnp.einsum('dhi,dhj->hij', whole_heads, whole_heads, preferred_element_ty...  5.61 us
    unnamed x19, local copies, waits for them, and re-layouts  4.7 us
  transfers between devices with their start and end apart: 2, of which 2 were waited for; matrix products, arithmetic and copies ran while one was open for 4% of the time, Pallas kernels for 0%

commit v1 on v0

--- a/solution.py
+++ b/solution.py
@@ -1,10 +1,16 @@
+import functools
+
 import jax
 import jax.numpy as jnp
 from jax import lax
+from jax.experimental import pallas as pl
+from jax.experimental.pallas import tpu as pltpu
 from jax.sharding import PartitionSpec as P
 
-
-def body(inputs, key_grads, weights, momentum, left_stat, right_stat, left_root, right_root):
+MESH = pl.DeviceIdType.MESH
+
+
+def plain_body(inputs, key_grads, weights, momentum, left_stat, right_stat, left_root, right_root):
     row_count = weights.shape[0]
     col_count = weights.shape[1]
     block_count = left_root.shape[0]
@@ -53,7 +59,270 @@
     return (momentum_next, left_next, right_next, update, weights_next, weights_copy)
 
 
+def kernel(
+    fs, tp, x_hbm, g_hbm, w_hbm, m_hbm, lroot_hbm, rroot_hbm,
+    step_ref, gram_ref, hgram_ref, wall_ref,
+    xv, gv, wv, mv, lroot, rroot, pbuf, crecv, ysend, yrecv, zsend, zrecv, whole, acc, grad_own, sc,
+    in_sem, x_sem, c_ss, c_rs, y_ss, y_rs, z_ss, z_rs, ag_ss, ag_rs, sc_ss, sc_rs,
+):
+    Y, Z = 2, fs // 4
+    chips = Y * Z
+    rows, cols = wv.shape
+    blocks = lroot.shape[0]
+    heads, hd = rroot.shape[0], rroot.shape[1]
+    bw = cols // blocks
+    f32, bf16 = jnp.float32, jnp.bfloat16
+    me = lax.axis_index("fs")
+    t = lax.axis_index("tp")
+    c = me % 2
+    y = (me // 2) % Y
+    z = me // (2 * Y)
+
+    def idx(zz, yy, cc):
+        return (zz * Y + yy) * 2 + cc
+
+    def remote(src, dst, ss, rs, peer):
+        cp = pltpu.make_async_remote_copy(
+            src_ref=src, dst_ref=dst, send_sem=ss, recv_sem=rs,
+            device_id=(peer, t), device_id_type=MESH,
+        )
+        cp.start()
+        return cp
+
+    partner = idx(z, y, 1 - c)
+    ypeer = idx(z, 1 - y, c)
+    zpeer = [idx((z + d) % Z, y, c) for d in range(1, Z)]
+
+    gcp = pltpu.make_async_copy(g_hbm, gv, in_sem.at[0])
+    gcp.start()
+    order = []
+    for i in range(chips):
+        yy = (y + 1 + i // Z) % Y
+        zz = (z + 1 + i) % Z
+        order.append(zz * Y + yy)
+    xcp = []
+    for i in range(chips):
+        start = pl.multiple_of(order[i] * (2 * rows), 2 * rows)
+        cp = pltpu.make_async_copy(x_hbm.at[:, pl.ds(start, 2 * rows)], xv.at[i], x_sem.at[i])
+        cp.start()
+        xcp.append(cp)
+    side = []
+    for k, (a, b) in enumerate(((lroot_hbm, lroot), (rroot_hbm, rroot), (w_hbm, wv), (m_hbm, mv))):
+        cp = pltpu.make_async_copy(a, b, in_sem.at[k + 1])
+        cp.start()
+        side.append(cp)
+
+    barrier = pltpu.get_barrier_semaphore()
+    total = fs * tp
+    linear = t * fs + me
+
+    @pl.loop(1, total)
+    def _(k):
+        other = (linear + k) % total
+        pl.semaphore_signal(
+            barrier, inc=1, device_id=(other % fs, other // fs), device_id_type=MESH
+        )
+
+    pl.semaphore_wait(barrier, total - 1)
+
+    ccp, ycp, zcp = [], [], []
+
+    def combine(i):
+        ccp[i].wait_recv()
+        s = pbuf[i, c] + crecv[i]
+        if i < Z:
+            ysend[i] = s.astype(bf16)
+            ycp.append(remote(ysend.at[i], yrecv.at[i], y_ss.at[i], y_rs.at[i], ypeer))
+        else:
+            crecv[i] = s
+
+    def zstage(j):
+        ycp[j].wait_recv()
+        s = crecv[Z + j] + yrecv[j].astype(f32)
+        if j < Z - 1:
+            zsend[j] = s.astype(bf16)
+            zcp.append(remote(zsend.at[j], zrecv.at[j], z_ss.at[j], z_rs.at[j], zpeer[j]))
+        else:
+            for k in range(Z - 1):
+                zcp[k].wait_recv()
+                s = s + zrecv[k].astype(f32)
+            grad_own[...] = s
+            whole[me] = s.astype(bf16)
+
+    gcp.wait()
+    for i in range(chips):
+        xcp[i].wait()
+        for half in range(2):
+            pbuf[i, half] = lax.dot_general(
+                xv[i, :, half * rows:(half + 1) * rows], gv[...],
+                (((0,), (0,)), ((), ())), preferred_element_type=f32,
+            )
+        ccp.append(remote(pbuf.at[i, 1 - c], crecv.at[i], c_ss.at[i], c_rs.at[i], partner))
+        if i > 0:
+            combine(i - 1)
+    combine(chips - 1)
+    for j in range(Z):
+        zstage(j)
+
+    def gather(buf, phase, use):
+        sends = []
+
+        def send(f, slot, peer):
+            cp = remote(buf.at[f], buf.at[f], ag_ss.at[phase, slot], ag_rs.at[phase, slot], peer)
+            sends.append(cp)
+
+        def arrived(f, slot):
+            pltpu.make_async_remote_copy(
+                src_ref=buf.at[f], dst_ref=buf.at[f], send_sem=ag_ss.at[phase, slot],
+                recv_sem=ag_rs.at[phase, slot], device_id=(ypeer, t), device_id_type=MESH,
+            ).wait_recv()
+
+        y0, c0 = Z - 1, 2 * Z - 1
+        send(me, y0, ypeer)
+        for d in range(1, Z):
+            send(me, d - 1, zpeer[d - 1])
+        send(me, c0, partner)
+        use(me)
+        for d in range(1, Z):
+            f = idx((z + Z - d) % Z, y, c)
+            arrived(f, d - 1)
+            send(f, y0 + d, ypeer)
+            send(f, c0 + d, partner)
+            use(f)
+        for d in range(Z):
+            f = idx((z + Z - d) % Z, 1 - y, c)
+            arrived(f, y0 + d)
+            send(f, c0 + Z + d, partner)
+            use(f)
+        for k in range(2 * Z):
+            yy = y if k < Z else 1 - y
+            f = idx((z + Z - k) % Z, yy, 1 - c)
+            arrived(f, c0 + k)
+            use(f)
+        for cp in sends:
+            cp.wait_send()
+
+    for cp in side:
+        cp.wait()
+    acc[...] = jnp.zeros_like(acc)
+
+    def use_grad(f):
+        at = pl.ds(pl.multiple_of(f * rows, rows), rows)
+        for b in range(blocks):
+            acc[:, b * bw:(b + 1) * bw] += jnp.dot(
+                lroot[b, :, at], whole[f, :, b * bw:(b + 1) * bw], preferred_element_type=f32
+            )
+
+    gather(whole, 0, use_grad)
+
+    for h in range(heads):
+        part = acc[:, h * hd:(h + 1) * hd].astype(bf16)
+        step_ref[:, h * hd:(h + 1) * hd] = jnp.dot(part, rroot[h], preferred_element_type=f32)
+    g = grad_own[...]
+    p = step_ref[...]
+    line = lax.broadcasted_iota(jnp.int32, sc.shape[1:], 0)
+    sc[linear] = jnp.where(line < 4, jnp.sum(g * g), jnp.sum(p * p))
+
+    def scalar_copy(k):
+        other = (linear + k) % total
+        return pltpu.make_async_remote_copy(
+            src_ref=sc.at[linear], dst_ref=sc.at[linear], send_sem=sc_ss.at[k],
+            recv_sem=sc_rs.at[k], device_id=(other % fs, other // fs), device_id_type=MESH,
+        )
+
+    @pl.loop(1, total)
+    def _(k):
+        scalar_copy(k).start()
+
+    hgram_ref[...] = jnp.zeros_like(hgram_ref)
+
+    @pl.loop(0, fs)
+    def _(f):
+        at = pl.ds(pl.multiple_of(f * rows, rows), rows)
+        for b in range(blocks):
+            gram_ref[b, :, at] = lax.dot_general(
+                whole[me, :, b * bw:(b + 1) * bw], whole[f, :, b * bw:(b + 1) * bw],
+                (((1,), (1,)), ((), ())), preferred_element_type=f32,
+            )
+        for h in range(heads):
+            v = whole[f, :, h * hd:(h + 1) * hd]
+            hgram_ref[h] += lax.dot_general(
+                v, v, (((0,), (0,)), ((), ())), preferred_element_type=f32
+            )
+
+    @pl.loop(1, total)
+    def _(k):
+        scalar_copy(k).wait()
+
+    sums = jnp.sum(sc[...], axis=0)
+    scale = jnp.sqrt(sums[0:1, 0:1] / (sums[4:5, 0:1] + 1e-06))
+    step = scale * step_ref[...]
+    step_ref[...] = step
+    w = wv[...]
+    wall_ref[me] = (w - 0.25 * ((0.9 * mv[...] + step) + 0.4 * w)).astype(bf16)
+    gather(wall_ref, 1, lambda f: None)
+    for cp in ccp + ycp + zcp:
+        cp.wait_send()
+
+
+def fast_body(fs, tp, inputs, key_grads, weights, momentum, left_stat, right_stat, left_root, right_root):
+    rows, cols = weights.shape
+    tokens, width = inputs.shape
+    blocks = left_root.shape[0]
+    Y, Z = 2, fs // 4
+    chips = Y * Z
+    f32, bf16 = jnp.float32, jnp.bfloat16
+    vm = pltpu.VMEM
+    dma = pltpu.SemaphoreType.DMA
+    step, gram, hgram, wall = pl.pallas_call(
+        functools.partial(kernel, fs, tp),
+        out_shape=(
+            jax.ShapeDtypeStruct((rows, cols), f32),
+            jax.ShapeDtypeStruct((blocks, rows, width), f32),
+            jax.ShapeDtypeStruct(right_root.shape, f32),
+            jax.ShapeDtypeStruct((fs, rows, cols), bf16),
+        ),
+        in_specs=[pl.BlockSpec(memory_space=pl.ANY)] * 6,
+        out_specs=[pl.BlockSpec(memory_space=pltpu.VMEM)] * 4,
+        scratch_shapes=[
+            vm((chips, tokens, 2 * rows), bf16),
+            vm((tokens, cols), bf16),
+            vm((rows, cols), f32),
+            vm((rows, cols), f32),
+            vm(left_root.shape, bf16),
+            vm(right_root.shape, bf16),
+            vm((chips, 2, rows, cols), f32),
+            vm((chips, rows, cols), f32),
+            vm((Z, rows, cols), bf16),
+            vm((Z, rows, cols), bf16),
+            vm((Z - 1, rows, cols), bf16),
+            vm((Z - 1, rows, cols), bf16),
+            vm((fs, rows, cols), bf16),
+            vm((rows, cols), f32),
+            vm((rows, cols), f32),
+            vm((fs * tp, 8, 128), f32),
+            dma((5,)), dma((chips,)),
+            dma((chips,)), dma((chips,)),
+            dma((Z,)), dma((Z,)),
+            dma((Z - 1,)), dma((Z - 1,)),
+            dma((2, 4 * Z - 1)), dma((2, 4 * Z - 1)),
+            dma((fs * tp,)), dma((fs * tp,)),
+        ],
+        compiler_params=pltpu.CompilerParams(
+            collective_id=0, has_side_effects=True, vmem_limit_bytes=56 * 1024 * 1024
+        ),
+    )(inputs, key_grads, weights, momentum, left_root, right_root)
+    left_next = 0.95 * left_stat + 0.05 * gram
+    right_next = 0.95 * right_stat + 0.05 * hgram
+    momentum_next = 0.9 * momentum + step
+    update = -0.25 * (momentum_next + 0.4 * weights)
+    weights_next = weights + update
+    weights_copy = wall.reshape(width, cols)
+    return (momentum_next, left_next, right_next, update, weights_next, weights_copy)
+
+
 def solution(mesh):
+    fs, tp = mesh.shape["fs"], mesh.shape["tp"]
     in_specs = (
         P("fs", None),
         P("fs", "tp"),
@@ -72,4 +341,11 @@
         P("fs", "tp"),
         P(None, "tp"),
     )
+
+    def body(inputs, *rest):
+        rows = inputs.shape[1] // fs
+        if fs % 4 == 0 and fs >= 8 and rows % 128 == 0:
+            return fast_body(fs, tp, inputs, *rest)
+        return plain_body(inputs, *rest)
+
     return jax.shard_map(body, mesh=mesh, in_specs=in_specs, out_specs=out_specs, check_vma=False)

time: 233 us -> 88 us (0.38)
  waiting for transfers between devices: 147 us -> 0 us
  Pallas kernels: 0 us -> 78.5 us
  blocking collectives: 39.7 us -> 0 us
  matrix products: 19.4 us -> 0 us
  between operations: 15.5 us -> 0.69 us
  local copies, waits for them, and re-layouts: 5.87 us -> 1.34 us
    psum x1 -> x0, waiting for transfers between devices: 114 us -> none  [body(): summed = lax.psum(partial_grad, 'fs')]
    pallas_call x0 -> x1, Pallas kernels: none -> 78.5 us  [fast_body(): pl.pallas_call(functools.partial(kernel, fs, tp), out_shape=(jax.ShapeDty...]
    psum x1 -> x0, blocking collectives: 39.7 us -> none  [body(): lax.psum((jnp.sum(grad * grad), jnp.sum(precond * precond)), ('fs', 'tp'))]
    all_gather x1 -> x0, waiting for transfers between devices: 32.6 us -> none  [body(): lax.all_gather(weights_next.astype(jnp.bfloat16), 'fs', axis=0, tiled=True)]
    dot_general x5 -> x0, matrix products: 19.4 us -> none  [the longest x1 9.81 us: body(): lax.dot_general(inputs, key_grads, (((0,), (0,)), ((), ())), preferred_el...]
    add x0 -> x3, other arithmetic: none -> 7.22 us  [the longest x1 3.46 us: fast_body(): left_next = 0.95 * left_stat + 0.05 * gram]
    convert_element_type x2 -> x0, other arithmetic: 3.57 us -> none  [the longest x1 2.54 us: body(): whole_bf = summed.astype(jnp.bfloat16)]
    unnamed x19 -> x11, local copies, waits for them, and re-layouts: 4.7 us -> 1.34 us
  transfers between devices with their start and end apart: 2 -> 0, of which waited for: 2 -> 0; matrix products, arithmetic and copies ran while one was open for 4% -> 0% of each run, Pallas kernels for 0% -> 0%
where the time goes in v1:
time: 88 us; the launch traced here: 87.8 us
  Pallas kernels  78.5 us (89%)
  other arithmetic  7.22 us (8%)
  local copies, waits for them, and re-layouts  1.34 us (2%)
    pallas_call x1, Pallas kernels, fast_body(): pl.pallas_call(functools.partial(kernel, fs, tp), out_shape=(jax.ShapeDty...  78.5 us
    add x1, other arithmetic, fast_body(): left_next = 0.95 * left_stat + 0.05 * gram  3.46 us
    add x1, other arithmetic, fast_body(): weights_next = weights + update  1.92 us
    add x1, other arithmetic, fast_body(): right_next = 0.95 * right_stat + 0.05 * hgram  1.84 us

profile of v1, /device:TPU:0, one launch (start us, length us, event | category | flops | bytes accessed | tf_op | source)
XLA Modules:
  0.0 87.8 jit_solution(15999792107489761285)
XLA Ops:
  0.6 0.0 copy-start.3
  0.6 0.0 copy-start.2
  0.7 0.0 copy-start.4
  0.7 78.5 %shard_map.127 = (f32[128,512]{1,0:T(8,128)}, f32[2,128,2048]{2,1,0:T(8,128)}, f32[4,128,128]{2,1,0:T(8,128)}, bf16[16,128,512]{2,1,0:T(8,128)(2,1)}) custom-call(bf16[2048,2048]{1,0:T(8,128)(2,1)} %x_hbm.1, bf16[2048,512]{1,0:T(8,128)(2,1)} %g_hbm.1, f32[128,512]{1,0:T(8,128)} %w_hbm.1, f32[128,512]{1,0:T(8,128)} %m_hbm.1, bf16[2,128,2048]{2,1,0:T(8,128)(2,1)} %lroot_hbm.1, ...), custom_call_target="tpu_custom_call" | custom-call | tf_op jit(solution)/shard_map/pallas_call | solution.py:277
  79.2 0.0 copy-start
  79.2 0.0 copy-done.4
  79.2 1.8 %multiply_add_fusion.1 = f32[4,128,128]{2,1,0:T(8,128)} fusion(f32[4,128,128]{2,1,0:T(8,128)} %get-tuple-element.12, f32[4,128,128]{2,1,0:T(8,128)S(1)} %copy-done.4), kind=kLoop, calls=%fused_computation.2 | loop fusion | flops 196608 | bytes 786432 | tf_op jit(solution)/shard_map/add | solution.py:316
  81.0 0.0 copy-done.3
  81.0 0.0 copy-done.2
  81.0 1.9 %fusion = (f32[128,512]{1,0:T(8,128)}, f32[128,512]{1,0:T(8,128)}, f32[128,512]{1,0:T(8,128)}) fusion(f32[128,512]{1,0:T(8,128)S(1)} %copy-done.2, f32[128,512]{1,0:T(8,128)} %get-tuple-element.10, f32[128,512]{1,0:T(8,128)S(1)} %copy-done.3), kind=kLoop, calls=%fused_computation.4 | loop fusion | flops 393216 | bytes 1572864 | tf_op jit(solution)/shard_map/add | solution.py:319
  83.0 0.0 copy-done
  83.0 0.0 copy-start.1
  83.0 3.5 %multiply_add_fusion = f32[2,128,2048]{2,1,0:T(8,128)} fusion(f32[2,128,2048]{2,1,0:T(8,128)} %get-tuple-element.11, f32[2,128,2048]{2,1,0:T(8,128)S(1)} %copy-done), kind=kLoop, calls=%fused_computation | loop fusion | flops 1572864 | bytes 6291456 | tf_op jit(solution)/shard_map/add | solution.py:315
  86.4 0.0 copy-done.1
  86.4 1.3 %copy.15 = bf16[2048,512]{1,0:T(8,128)(2,1)} copy(bf16[2048,512]{1,0:T(8,128)(2,1)S(1)} %bitcast.1) | data formatting | bytes 4194304
Async XLA Ops:
  0.6 80.4 %copy-start.3 = (f32[128,512]{1,0:T(8,128)S(1)}, f32[128,512]{1,0:T(8,128)}, u32[]{:S(2)}) copy-start(f32[128,512]{1,0:T(8,128)} %m_hbm.1) | copy-start | bytes 786436
  0.6 80.4 %copy-start.2 = (f32[128,512]{1,0:T(8,128)S(1)}, f32[128,512]{1,0:T(8,128)}, u32[]{:S(2)}) copy-start(f32[128,512]{1,0:T(8,128)} %w_hbm.1) | copy-start | bytes 786436
  0.7 78.5 %copy-start.4 = (f32[4,128,128]{2,1,0:T(8,128)S(1)}, f32[4,128,128]{2,1,0:T(8,128)}, u32[]{:S(2)}) copy-start(f32[4,128,128]{2,1,0:T(8,128)} %param.13) | copy-start | bytes 786436
  79.2 3.8 %copy-start = (f32[2,128,2048]{2,1,0:T(8,128)S(1)}, f32[2,128,2048]{2,1,0:T(8,128)}, u32[]{:S(2)}) copy-start(f32[2,128,2048]{2,1,0:T(8,128)} %param.12) | copy-start | bytes 6291460
  83.0 3.5 %copy-start.1 = (bf16[16,128,512]{2,1,0:T(8,128)(2,1)S(1)}, bf16[16,128,512]{2,1,0:T(8,128)(2,1)}, u32[]{:S(2)}) copy-start(bf16[16,128,512]{2,1,0:T(8,128)(2,1)} %get-tuple-element.13) | copy-start | bytes 6291460

commit v2 on v1

--- a/solution.py
+++ b/solution.py
@@ -63,7 +63,7 @@
     fs, tp, x_hbm, g_hbm, w_hbm, m_hbm, lroot_hbm, rroot_hbm,
     step_ref, gram_ref, hgram_ref, wall_ref,
     xv, gv, wv, mv, lroot, rroot, pbuf, crecv, ysend, yrecv, zsend, zrecv, whole, acc, grad_own, sc,
-    in_sem, x_sem, c_ss, c_rs, y_ss, y_rs, z_ss, z_rs, ag_ss, ag_rs, sc_ss, sc_rs,
+    in_sem, x_sem, c_ss, c_rs, y_ss, y_rs, z_ss, z_rs, gu_ss, gd_ss, gz_rs, gy_ss, gy_rs, gc_ss, gc_rs, sc_ss, sc_rs,
 ):
     Y, Z = 2, fs // 4
     chips = Y * Z
@@ -123,8 +123,6 @@
             barrier, inc=1, device_id=(other % fs, other // fs), device_id_type=MESH
         )
 
-    pl.semaphore_wait(barrier, total - 1)
-
     ccp, ycp, zcp = [], [], []
 
     def combine(i):
@@ -157,6 +155,8 @@
                 xv[i, :, half * rows:(half + 1) * rows], gv[...],
                 (((0,), (0,)), ((), ())), preferred_element_type=f32,
             )
+        if i == 0:
+            pl.semaphore_wait(barrier, total - 1)
         ccp.append(remote(pbuf.at[i, 1 - c], crecv.at[i], c_ss.at[i], c_rs.at[i], partner))
         if i > 0:
             combine(i - 1)
@@ -164,43 +164,89 @@
     for j in range(Z):
         zstage(j)
 
-    def gather(buf, phase, use):
-        sends = []
-
-        def send(f, slot, peer):
-            cp = remote(buf.at[f], buf.at[f], ag_ss.at[phase, slot], ag_rs.at[phase, slot], peer)
-            sends.append(cp)
-
-        def arrived(f, slot):
+    hr = rows // 2
+    halves = range(2)
+
+    def gather(buf, ph, use, filler):
+        def copy(kind, q, h):
+            if kind == "c":
+                f, peer, ss, rs = 2 * q + c, partner, gc_ss, gc_rs
+            elif kind == "y":
+                f, peer, ss, rs = idx(q, y, c), ypeer, gy_ss, gy_rs
+            else:
+                up = kind == "u"
+                f, peer = idx(q, y, c), idx(lax.rem(z + (1 if up else Z - 1), Z), y, c)
+                ss, rs = gu_ss if up else gd_ss, gz_rs
+            part = buf.at[f, pl.ds(h * hr, hr)]
+            return pltpu.make_async_remote_copy(
+                src_ref=part, dst_ref=part, send_sem=ss.at[ph, h, q], recv_sem=rs.at[ph, h, q],
+                device_id=(peer, t), device_id_type=MESH,
+            )
+
+        def arrived(kind, q, h):
+            if kind == "c":
+                f, ss, rs = 2 * q + 1 - c, gc_ss, gc_rs
+            elif kind == "y":
+                f, ss, rs = idx(q, 1 - y, c), gy_ss, gy_rs
+            else:
+                f, ss, rs = idx(q, y, c), gu_ss, gz_rs
+            part = buf.at[f, pl.ds(h * hr, hr)]
             pltpu.make_async_remote_copy(
-                src_ref=buf.at[f], dst_ref=buf.at[f], send_sem=ag_ss.at[phase, slot],
-                recv_sem=ag_rs.at[phase, slot], device_id=(ypeer, t), device_id_type=MESH,
+                src_ref=part, dst_ref=part, send_sem=ss.at[ph, h, q], recv_sem=rs.at[ph, h, q],
+                device_id=(partner, t), device_id_type=MESH,
             ).wait_recv()
 
-        y0, c0 = Z - 1, 2 * Z - 1
-        send(me, y0, ypeer)
-        for d in range(1, Z):
-            send(me, d - 1, zpeer[d - 1])
-        send(me, c0, partner)
+        def spread(q, h, up, down):
+            if up:
+                @pl.when(z < Z - 1)
+                def _():
+                    copy("u", q, h).start()
+            if down:
+                @pl.when(z > 0)
+                def _():
+                    copy("d", q, h).start()
+            copy("y", q, h).start()
+            copy("c", q * Y + y, h).start()
+
+        for h in halves:
+            spread(z, h, True, True)
         use(me)
-        for d in range(1, Z):
-            f = idx((z + Z - d) % Z, y, c)
-            arrived(f, d - 1)
-            send(f, y0 + d, ypeer)
-            send(f, c0 + d, partner)
-            use(f)
-        for d in range(Z):
-            f = idx((z + Z - d) % Z, 1 - y, c)
-            arrived(f, y0 + d)
-            send(f, c0 + Z + d, partner)
-            use(f)
-        for k in range(2 * Z):
-            yy = y if k < Z else 1 - y
-            f = idx((z + Z - k) % Z, yy, 1 - c)
-            arrived(f, c0 + k)
-            use(f)
-        for cp in sends:
-            cp.wait_send()
+        filler(0)
+        for j in range(1, Z):
+            for below in (True, False):
+                @pl.when(z - j >= 0 if below else z + j < Z)
+                def _(j=j, below=below):
+                    q = z - j if below else z + j
+                    for h in halves:
+                        arrived("z", q, h)
+                        spread(q, h, below, not below)
+                    use(idx(q, y, c))
+            filler(j)
+        for j in range(Z):
+            q = (z + j) % Z
+            for h in halves:
+                arrived("y", q, h)
+                copy("c", q * Y + 1 - y, h).start()
+            use(idx(q, 1 - y, c))
+        for j in range(Z):
+            for yy in (y, 1 - y):
+                q = (z + j) % Z * Y + yy
+                for h in halves:
+                    arrived("c", q, h)
+                use(2 * q + 1 - c)
+        for h in halves:
+            for q in range(Z):
+                @pl.when((z < Z - 1) & (q <= z))
+                def _(q=q, h=h):
+                    copy("u", q, h).wait_send()
+
+                @pl.when((z > 0) & (q >= z))
+                def _(q=q, h=h):
+                    copy("d", q, h).wait_send()
+
+                copy("y", q, h).wait_send()
+            for q in range(chips):
+                copy("c", q, h).wait_send()
 
     for cp in side:
         cp.wait()
@@ -213,7 +259,7 @@
                 lroot[b, :, at], whole[f, :, b * bw:(b + 1) * bw], preferred_element_type=f32
             )
 
-    gather(whole, 0, use_grad)
+    gather(whole, 0, use_grad, lambda j: None)
 
     for h in range(heads):
         part = acc[:, h * hd:(h + 1) * hd].astype(bf16)
@@ -236,19 +282,20 @@
 
     hgram_ref[...] = jnp.zeros_like(hgram_ref)
 
-    @pl.loop(0, fs)
-    def _(f):
-        at = pl.ds(pl.multiple_of(f * rows, rows), rows)
-        for b in range(blocks):
-            gram_ref[b, :, at] = lax.dot_general(
-                whole[me, :, b * bw:(b + 1) * bw], whole[f, :, b * bw:(b + 1) * bw],
-                (((1,), (1,)), ((), ())), preferred_element_type=f32,
-            )
-        for h in range(heads):
-            v = whole[f, :, h * hd:(h + 1) * hd]
-            hgram_ref[h] += lax.dot_general(
-                v, v, (((0,), (0,)), ((), ())), preferred_element_type=f32
-            )
+    def grams(j):
+        @pl.loop(j * (fs // Z), (j + 1) * (fs // Z))
+        def _(f):
+            at = pl.ds(pl.multiple_of(f * rows, rows), rows)
+            for b in range(blocks):
+                gram_ref[b, :, at] = lax.dot_general(
+                    whole[me, :, b * bw:(b + 1) * bw], whole[f, :, b * bw:(b + 1) * bw],
+                    (((1,), (1,)), ((), ())), preferred_element_type=f32,
+                )
+            for h in range(heads):
+                v = whole[f, :, h * hd:(h + 1) * hd]
+                hgram_ref[h] += lax.dot_general(
+                    v, v, (((0,), (0,)), ((), ())), preferred_element_type=f32
+                )
 
     @pl.loop(1, total)
     def _(k):
@@ -260,7 +307,7 @@
     step_ref[...] = step
     w = wv[...]
     wall_ref[me] = (w - 0.25 * ((0.9 * mv[...] + step) + 0.4 * w)).astype(bf16)
-    gather(wall_ref, 1, lambda f: None)
+    gather(wall_ref, 1, lambda f: None, grams)
     for cp in ccp + ycp + zcp:
         cp.wait_send()
 
@@ -282,7 +329,7 @@
             jax.ShapeDtypeStruct(right_root.shape, f32),
             jax.ShapeDtypeStruct((fs, rows, cols), bf16),
         ),
-        in_specs=[pl.BlockSpec(memory_space=pl.ANY)] * 6,
+        in_specs=[pl.BlockSpec(memory_space=pltpu.HBM)] * 6,
         out_specs=[pl.BlockSpec(memory_space=pltpu.VMEM)] * 4,
         scratch_shapes=[
             vm((chips, tokens, 2 * rows), bf16),
@@ -305,11 +352,13 @@
             dma((chips,)), dma((chips,)),
             dma((Z,)), dma((Z,)),
             dma((Z - 1,)), dma((Z - 1,)),
-            dma((2, 4 * Z - 1)), dma((2, 4 * Z - 1)),
+            dma((2, 2, Z)), dma((2, 2, Z)), dma((2, 2, Z)),
+            dma((2, 2, Z)), dma((2, 2, Z)),
+            dma((2, 2, chips)), dma((2, 2, chips)),
             dma((fs * tp,)), dma((fs * tp,)),
         ],
         compiler_params=pltpu.CompilerParams(
-            collective_id=0, has_side_effects=True, vmem_limit_bytes=56 * 1024 * 1024
+            collective_id=0, has_side_effects=True, vmem_limit_bytes=30 * 1024 * 1024
         ),
     )(inputs, key_grads, weights, momentum, left_root, right_root)
     left_next = 0.95 * left_stat + 0.05 * gram

time: 88 us -> 85.6 us (0.973)
  local copies, waits for them, and re-layouts: 1.34 us -> 10.3 us
  Pallas kernels: 78.5 us -> 70.9 us
  other arithmetic: 7.22 us -> 3.44 us
    unnamed x11 -> x17, local copies, waits for them, and re-layouts: 1.34 us -> 10.3 us
    pallas_call x1, Pallas kernels: 78.5 us -> 70.9 us  [fast_body(): pl.pallas_call(functools.partial(kernel, fs, tp), out_shape=(jax.ShapeDty...]
    add x1, other arithmetic: 3.46 us -> 1.73 us  [fast_body(): left_next = 0.95 * left_stat + 0.05 * gram]
    add x1, other arithmetic: 1.84 us -> 0.75 us  [fast_body(): right_next = 0.95 * right_stat + 0.05 * hgram]
    add x1, other arithmetic: 1.92 us -> 0.97 us  [fast_body(): weights_next = weights + update]
where the time goes in v2:
time: 85.6 us; the launch traced here: 85.3 us
  Pallas kernels  70.9 us (83%)
  local copies, waits for them, and re-layouts  10.3 us (12%)
  other arithmetic  3.44 us (4%)
    pallas_call x1, Pallas kernels, fast_body(): pl.pallas_call(functools.partial(kernel, fs, tp), out_shape=(jax.ShapeDty...  70.9 us
    unnamed x17, local copies, waits for them, and re-layouts  10.3 us
    add x1, other arithmetic, fast_body(): left_next = 0.95 * left_stat + 0.05 * gram  1.73 us

profile of v2, /device:TPU:0, one launch (start us, length us, event | category | flops | bytes accessed | tf_op | source)
XLA Modules:
  0.0 85.3 jit_solution(5141551238151653863)
XLA Ops:
  0.6 0.0 copy-start
  0.6 3.4 %copy-done = bf16[2048,2048]{1,0:T(8,128)(2,1)S(1)} copy-done((bf16[2048,2048]{1,0:T(8,128)(2,1)S(1)}, bf16[2048,2048]{1,0:T(8,128)(2,1)}, u32[]{:S(2)}) %copy-start) | copy-done | bytes 8388632
  4.0 0.0 copy-start.1
  4.0 1.6 %copy-done.1 = bf16[2048,512]{1,0:T(8,128)(2,1)S(1)} copy-done((bf16[2048,512]{1,0:T(8,128)(2,1)S(1)}, bf16[2048,512]{1,0:T(8,128)(2,1)}, u32[]{:S(2)}) %copy-start.1) | copy-done | bytes 2097176
  5.6 0.0 copy-start.2
  5.6 1.2 %copy-done.2 = bf16[2,128,2048]{2,1,0:T(8,128)(2,1)S(1)} copy-done((bf16[2,128,2048]{2,1,0:T(8,128)(2,1)S(1)}, bf16[2,128,2048]{2,1,0:T(8,128)(2,1)}, u32[]{:S(2)}) %copy-start.2) | copy-done | bytes 1048600
  6.8 0.0 copy-start.3
  6.8 0.9 %copy-done.3 = f32[128,512]{1,0:T(8,128)S(1)} copy-done((f32[128,512]{1,0:T(8,128)S(1)}, f32[128,512]{1,0:T(8,128)}, u32[]{:S(2)}) %copy-start.3) | copy-done | bytes 262168
  7.8 0.0 copy-start.4
  7.8 0.9 %copy-done.4 = f32[128,512]{1,0:T(8,128)S(1)} copy-done((f32[128,512]{1,0:T(8,128)S(1)}, f32[128,512]{1,0:T(8,128)}, u32[]{:S(2)}) %copy-start.4) | copy-done | bytes 262168
  8.7 0.0 copy-start.5
  8.7 0.9 %copy-done.5 = bf16[4,128,128]{2,1,0:T(8,128)(2,1)S(1)} copy-done((bf16[4,128,128]{2,1,0:T(8,128)(2,1)S(1)}, bf16[4,128,128]{2,1,0:T(8,128)(2,1)}, u32[]{:S(2)}) %copy-start.5) | copy-done | bytes 131096
  9.6 0.0 copy-start.7
  9.6 70.9 %shard_map.127 = (f32[128,512]{1,0:T(8,128)S(1)}, f32[2,128,2048]{2,1,0:T(8,128)S(1)}, f32[4,128,128]{2,1,0:T(8,128)S(1)}, bf16[16,128,512]{2,1,0:T(8,128)(2,1)S(1)}) custom-call(bf16[2048,2048]{1,0:T(8,128)(2,1)S(1)} %copy-done, bf16[2048,512]{1,0:T(8,128)(2,1)S(1)} %copy-done.1, f32[128,512]{1,0:T(8,128)S(1)} %copy-done.3, f32[128,512]{1,0:T(8,128)S(1)} %copy-done.4, ...), custom_call_target="tpu_custom_call" | custom-call | tf_op jit(solution)/shard_map/pallas_call | solution.py:324
  80.6 0.0 copy-start.6
  80.6 0.0 copy-done.7
  80.6 0.7 multiply_add_fusion.1
  81.3 1.0 %fusion = (f32[128,512]{1,0:T(8,128)}, f32[128,512]{1,0:T(8,128)}, f32[128,512]{1,0:T(8,128)}) fusion(f32[128,512]{1,0:T(8,128)S(1)} %copy-done.3, f32[128,512]{1,0:T(8,128)S(1)} %get-tuple-element.10, f32[128,512]{1,0:T(8,128)S(1)} %copy-done.4), kind=kLoop, calls=%fused_computation.4 | loop fusion | flops 393216 | bytes 1572864 | tf_op jit(solution)/shard_map/add | solution.py:368
  82.3 0.0 copy-done.6
  82.3 1.7 %multiply_add_fusion = f32[2,128,2048]{2,1,0:T(8,128)} fusion(f32[2,128,2048]{2,1,0:T(8,128)S(1)} %get-tuple-element.11, f32[2,128,2048]{2,1,0:T(8,128)S(1)} %copy-done.6), kind=kLoop, calls=%fused_computation | loop fusion | flops 1572864 | bytes 6291456 | tf_op jit(solution)/shard_map/add | solution.py:364
  84.0 1.3 %copy.15 = bf16[2048,512]{1,0:T(8,128)(2,1)} copy(bf16[2048,512]{1,0:T(8,128)(2,1)S(1)} %bitcast.1) | data formatting | bytes 4194304
Async XLA Ops:
  0.6 3.4 %copy-start = (bf16[2048,2048]{1,0:T(8,128)(2,1)S(1)}, bf16[2048,2048]{1,0:T(8,128)(2,1)}, u32[]{:S(2)}) copy-start(bf16[2048,2048]{1,0:T(8,128)(2,1)} %x_hbm.1) | copy-start | bytes 25165828
  4.0 1.6 %copy-start.1 = (bf16[2048,512]{1,0:T(8,128)(2,1)S(1)}, bf16[2048,512]{1,0:T(8,128)(2,1)}, u32[]{:S(2)}) copy-start(bf16[2048,512]{1,0:T(8,128)(2,1)} %g_hbm.1) | copy-start | bytes 6291460
  5.6 1.2 %copy-start.2 = (bf16[2,128,2048]{2,1,0:T(8,128)(2,1)S(1)}, bf16[2,128,2048]{2,1,0:T(8,128)(2,1)}, u32[]{:S(2)}) copy-start(bf16[2,128,2048]{2,1,0:T(8,128)(2,1)} %lroot_hbm.1) | copy-start | bytes 3145732
  6.8 0.9 %copy-start.3 = (f32[128,512]{1,0:T(8,128)S(1)}, f32[128,512]{1,0:T(8,128)}, u32[]{:S(2)}) copy-start(f32[128,512]{1,0:T(8,128)} %w_hbm.1) | copy-start | bytes 786436
  7.8 0.9 %copy-start.4 = (f32[128,512]{1,0:T(8,128)S(1)}, f32[128,512]{1,0:T(8,128)}, u32[]{:S(2)}) copy-start(f32[128,512]{1,0:T(8,128)} %m_hbm.1) | copy-start | bytes 786436
  8.7 0.9 %copy-start.5 = (bf16[4,128,128]{2,1,0:T(8,128)(2,1)S(1)}, bf16[4,128,128]{2,1,0:T(8,128)(2,1)}, u32[]{:S(2)}) copy-start(bf16[4,128,128]{2,1,0:T(8,128)(2,1)} %rroot_hbm.1) | copy-start | bytes 393220
  9.6 70.9 %copy-start.7 = (f32[4,128,128]{2,1,0:T(8,128)S(1)}, f32[4,128,128]{2,1,0:T(8,128)}, u32[]{:S(2)}) copy-start(f32[4,128,128]{2,1,0:T(8,128)} %param.13) | copy-start | bytes 786436
  80.6 1.7 %copy-start.6 = (f32[2,128,2048]{2,1,0:T(8,128)S(1)}, f32[2,128,2048]{2,1,0:T(8,128)}, u32[]{:S(2)}) copy-start(f32[2,128,2048]{2,1,0:T(8,128)} %param.12) | copy-start | bytes 6291460

commit v3 on v2

--- a/solution.py
+++ b/solution.py
@@ -321,6 +321,7 @@
     f32, bf16 = jnp.float32, jnp.bfloat16
     vm = pltpu.VMEM
     dma = pltpu.SemaphoreType.DMA
+    operands = (inputs, key_grads, weights, momentum, left_root, right_root)
     step, gram, hgram, wall = pl.pallas_call(
         functools.partial(kernel, fs, tp),
         out_shape=(
@@ -360,7 +361,7 @@
         compiler_params=pltpu.CompilerParams(
             collective_id=0, has_side_effects=True, vmem_limit_bytes=30 * 1024 * 1024
         ),
-    )(inputs, key_grads, weights, momentum, left_root, right_root)
+    )(*(pltpu.with_memory_space_constraint(a, pltpu.HBM) for a in operands))
     left_next = 0.95 * left_stat + 0.05 * gram
     right_next = 0.95 * right_stat + 0.05 * hgram
     momentum_next = 0.9 * momentum + step

time: 85.6 us -> 76.2 us (0.89)
  local copies, waits for them, and re-layouts: 10.3 us -> 1.34 us
    unnamed x17 -> x9, local copies, waits for them, and re-layouts: 10.3 us -> 1.34 us
where the time goes in v3:
time: 76.2 us; the launch traced here: 76 us
  Pallas kernels  70.5 us (93%)
  other arithmetic  3.45 us (5%)
  local copies, waits for them, and re-layouts  1.34 us (2%)
    pallas_call x1, Pallas kernels, fast_body(): pl.pallas_call(functools.partial(kernel, fs, tp), out_shape=(jax.ShapeDty...  70.5 us
    add x1, other arithmetic, fast_body(): left_next = 0.95 * left_stat + 0.05 * gram  1.73 us

profile of v3, /device:TPU:0, one launch (start us, length us, event | category | flops | bytes accessed | tf_op | source)
XLA Modules:
  0.0 76.0 jit_solution(9712837729829071025)
XLA Ops:
  0.6 0.0 copy-start.2
  0.6 0.0 copy-start.1
  0.7 0.0 copy-start.3
  0.7 70.5 %shard_map.127 = (f32[128,512]{1,0:T(8,128)S(1)}, f32[2,128,2048]{2,1,0:T(8,128)S(1)}, f32[4,128,128]{2,1,0:T(8,128)S(1)}, bf16[16,128,512]{2,1,0:T(8,128)(2,1)S(1)}) custom-call(bf16[2048,2048]{1,0:T(8,128)(2,1)} %x_hbm.1, bf16[2048,512]{1,0:T(8,128)(2,1)} %g_hbm.1, f32[128,512]{1,0:T(8,128)} %w_hbm.1, f32[128,512]{1,0:T(8,128)} %m_hbm.1, ...), custom_call_target="tpu_custom_call" | custom-call | tf_op jit(solution)/shard_map/pallas_call | solution.py:325
  71.2 0.0 copy-start
  71.2 0.0 copy-done.3
  71.2 0.7 multiply_add_fusion.1
  72.0 0.0 copy-done.2
  72.0 0.0 copy-done.1
  72.0 1.0 %fusion = (f32[128,512]{1,0:T(8,128)}, f32[128,512]{1,0:T(8,128)}, f32[128,512]{1,0:T(8,128)}) fusion(f32[128,512]{1,0:T(8,128)S(1)} %copy-done.1, f32[128,512]{1,0:T(8,128)S(1)} %get-tuple-element.10, f32[128,512]{1,0:T(8,128)S(1)} %copy-done.2), kind=kLoop, calls=%fused_computation.4 | loop fusion | flops 393216 | bytes 1572864 | tf_op jit(solution)/shard_map/add | solution.py:369
  73.0 0.0 copy-done
  73.0 1.7 %multiply_add_fusion = f32[2,128,2048]{2,1,0:T(8,128)} fusion(f32[2,128,2048]{2,1,0:T(8,128)S(1)} %get-tuple-element.11, f32[2,128,2048]{2,1,0:T(8,128)S(1)} %copy-done), kind=kLoop, calls=%fused_computation | loop fusion | flops 1572864 | bytes 6291456 | tf_op jit(solution)/shard_map/add | solution.py:365
  74.7 1.3 %copy.15 = bf16[2048,512]{1,0:T(8,128)(2,1)} copy(bf16[2048,512]{1,0:T(8,128)(2,1)S(1)} %bitcast.1) | data formatting | bytes 4194304
Async XLA Ops:
  0.6 71.3 %copy-start.2 = (f32[128,512]{1,0:T(8,128)S(1)}, f32[128,512]{1,0:T(8,128)}, u32[]{:S(2)}) copy-start(f32[128,512]{1,0:T(8,128)} %m_hbm.1) | copy-start | bytes 786436
  0.6 71.3 %copy-start.1 = (f32[128,512]{1,0:T(8,128)S(1)}, f32[128,512]{1,0:T(8,128)}, u32[]{:S(2)}) copy-start(f32[128,512]{1,0:T(8,128)} %w_hbm.1) | copy-start | bytes 786436
  0.7 70.6 %copy-start.3 = (f32[4,128,128]{2,1,0:T(8,128)S(1)}, f32[4,128,128]{2,1,0:T(8,128)}, u32[]{:S(2)}) copy-start(f32[4,128,128]{2,1,0:T(8,128)} %param.13) | copy-start | bytes 786436
  71.2 1.7 %copy-start = (f32[2,128,2048]{2,1,0:T(8,128)S(1)}, f32[2,128,2048]{2,1,0:T(8,128)}, u32[]{:S(2)}) copy-start(f32[2,128,2048]{2,1,0:T(8,128)} %param.12) | copy-start | bytes 6291460

commit v4 on v3

--- a/solution.py
+++ b/solution.py
@@ -101,15 +101,16 @@
         zz = (z + 1 + i) % Z
         order.append(zz * Y + yy)
     xcp = []
+    ahead = 3
     for i in range(chips):
         start = pl.multiple_of(order[i] * (2 * rows), 2 * rows)
         cp = pltpu.make_async_copy(x_hbm.at[:, pl.ds(start, 2 * rows)], xv.at[i], x_sem.at[i])
-        cp.start()
+        if i < ahead:
+            cp.start()
         xcp.append(cp)
     side = []
     for k, (a, b) in enumerate(((lroot_hbm, lroot), (rroot_hbm, rroot), (w_hbm, wv), (m_hbm, mv))):
         cp = pltpu.make_async_copy(a, b, in_sem.at[k + 1])
-        cp.start()
         side.append(cp)
 
     barrier = pltpu.get_barrier_semaphore()
@@ -150,16 +151,20 @@
     gcp.wait()
     for i in range(chips):
         xcp[i].wait()
-        for half in range(2):
-            pbuf[i, half] = lax.dot_general(
-                xv[i, :, half * rows:(half + 1) * rows], gv[...],
-                (((0,), (0,)), ((), ())), preferred_element_type=f32,
-            )
+        if i + ahead < chips:
+            xcp[i + ahead].start()
+        both = lax.dot_general(
+            xv[i], gv[...], (((0,), (0,)), ((), ())), preferred_element_type=f32
+        )
+        pbuf[i, 0] = both[:rows]
+        pbuf[i, 1] = both[rows:]
         if i == 0:
             pl.semaphore_wait(barrier, total - 1)
         ccp.append(remote(pbuf.at[i, 1 - c], crecv.at[i], c_ss.at[i], c_rs.at[i], partner))
         if i > 0:
             combine(i - 1)
+    for cp in side:
+        cp.start()
     combine(chips - 1)
     for j in range(Z):
         zstage(j)

time: 76.2 us -> 75.9 us (level)
  no operation moved by 1% of the time
where the time goes in v4:
time: 75.9 us; the launch traced here: 75.7 us
  Pallas kernels  70.3 us (93%)
  other arithmetic  3.45 us (5%)
  local copies, waits for them, and re-layouts  1.34 us (2%)
    pallas_call x1, Pallas kernels, fast_body(): pl.pallas_call(functools.partial(kernel, fs, tp), out_shape=(jax.ShapeDty...  70.3 us
    add x1, other arithmetic, fast_body(): left_next = 0.95 * left_stat + 0.05 * gram  1.73 us

profile of v4, /device:TPU:0, one launch (start us, length us, event | category | flops | bytes accessed | tf_op | source)
XLA Modules:
  0.0 75.7 jit_solution(12432476885205825911)
XLA Ops:
  0.6 0.0 copy-start.2
  0.6 0.0 copy-start.1
  0.7 0.0 copy-start.3
  0.7 70.3 %shard_map.127 = (f32[128,512]{1,0:T(8,128)S(1)}, f32[2,128,2048]{2,1,0:T(8,128)S(1)}, f32[4,128,128]{2,1,0:T(8,128)S(1)}, bf16[16,128,512]{2,1,0:T(8,128)(2,1)S(1)}) custom-call(bf16[2048,2048]{1,0:T(8,128)(2,1)} %x_hbm.1, bf16[2048,512]{1,0:T(8,128)(2,1)} %g_hbm.1, f32[128,512]{1,0:T(8,128)} %w_hbm.1, f32[128,512]{1,0:T(8,128)} %m_hbm.1, ...), custom_call_target="tpu_custom_call" | custom-call | tf_op jit(solution)/shard_map/pallas_call | solution.py:330
  71.0 0.0 copy-start
  71.0 0.0 copy-done.3
  71.0 0.7 multiply_add_fusion.1
  71.7 0.0 copy-done.2
  71.7 0.0 copy-done.1
  71.7 1.0 %fusion = (f32[128,512]{1,0:T(8,128)}, f32[128,512]{1,0:T(8,128)}, f32[128,512]{1,0:T(8,128)}) fusion(f32[128,512]{1,0:T(8,128)S(1)} %copy-done.1, f32[128,512]{1,0:T(8,128)S(1)} %get-tuple-element.10, f32[128,512]{1,0:T(8,128)S(1)} %copy-done.2), kind=kLoop, calls=%fused_computation.4 | loop fusion | flops 393216 | bytes 1572864 | tf_op jit(solution)/shard_map/add | solution.py:374
  72.7 0.0 copy-done
  72.7 1.7 %multiply_add_fusion = f32[2,128,2048]{2,1,0:T(8,128)} fusion(f32[2,128,2048]{2,1,0:T(8,128)S(1)} %get-tuple-element.11, f32[2,128,2048]{2,1,0:T(8,128)S(1)} %copy-done), kind=kLoop, calls=%fused_computation | loop fusion | flops 1572864 | bytes 6291456 | tf_op jit(solution)/shard_map/add | solution.py:370
  74.4 1.3 %copy.15 = bf16[2048,512]{1,0:T(8,128)(2,1)} copy(bf16[2048,512]{1,0:T(8,128)(2,1)S(1)} %bitcast.1) | data formatting | bytes 4194304
Async XLA Ops:
  0.6 71.1 %copy-start.2 = (f32[128,512]{1,0:T(8,128)S(1)}, f32[128,512]{1,0:T(8,128)}, u32[]{:S(2)}) copy-start(f32[128,512]{1,0:T(8,128)} %m_hbm.1) | copy-start | bytes 786436
  0.6 71.1 %copy-start.1 = (f32[128,512]{1,0:T(8,128)S(1)}, f32[128,512]{1,0:T(8,128)}, u32[]{:S(2)}) copy-start(f32[128,512]{1,0:T(8,128)} %w_hbm.1) | copy-start | bytes 786436
  0.7 70.3 %copy-start.3 = (f32[4,128,128]{2,1,0:T(8,128)S(1)}, f32[4,128,128]{2,1,0:T(8,128)}, u32[]{:S(2)}) copy-start(f32[4,128,128]{2,1,0:T(8,128)} %param.13) | copy-start | bytes 786436
  71.0 1.7 %copy-start = (f32[2,128,2048]{2,1,0:T(8,128)S(1)}, f32[2,128,2048]{2,1,0:T(8,128)}, u32[]{:S(2)}) copy-start(f32[2,128,2048]{2,1,0:T(8,128)} %param.12) | copy-start | bytes 6291460
